TPU v7x, 32 devices: a whole 2x2x4 slice. The times are simulated.
32 devices in a mesh: sp: 8 (over z, y), tp: 4 (over x, core).
Axes of the slice: x: 2, y: 2, z: 4, core: 2. Of those that a mesh axis runs over, the one named last changes fastest.
Arguments:
- residual_in: bfloat16 [4096, 2048], P('sp'), may hold values from -6 to 6
- queries_nope: bfloat16 [4096, 1024], P('sp', 'tp'), may hold values from -15 to 15
- queries_rope: bfloat16 [4096, 512], P('sp', 'tp'), may hold values from -400 to 400
- latents: bfloat16 [4096, 256], P('sp'), may hold values from -6 to 6
- rope_keys: bfloat16 [4096, 32], P('sp'), may hold values from -8 to 8
- latent_norm_gain: float32 [256], replicated, may hold values from 0.1 to 1.9
- key_up_weight: bfloat16 [256, 1024], P(None, 'tp'), may hold values from -0.375 to 0.375
- value_up_weight: bfloat16 [256, 1024], P(None, 'tp'), may hold values from -0.375 to 0.375
- w_out: bfloat16 [1024, 2048], P('tp'), may hold values from -0.59765625 to 0.59765625
- norm_gain: float32 [2048], replicated, may hold values from 0.1 to 1.9
- w_up: bfloat16 [2048, 8192], P('sp', 'tp'), may hold values from -0.125 to 0.125
- w_down: bfloat16 [8192, 2048], P('tp', 'sp'), may hold values from -0.0625 to 0.0625
Outputs:
- layer_out: bfloat16 [4096, 2048], P('sp', 'tp')
All inputs are finite; a program needn't handle non-finite values.
Results may differ from a plain program's by a relative error of at most 0.015.
Values may be sent and summed in bfloat16 or wider, within the bound.
A program may use at most 128 MiB of HBM per device.

v0:
```python
import math
import jax
import jax.numpy as jnp
from jax import lax
from jax.sharding import PartitionSpec as P

UNROTATED_WIDTH = 64
ROPE = 32
rope_base = 10000.0
epsilon = 1e-06


def rotate(vectors, phases):
    half_width = vectors.shape[-1] // 2
    first_half = vectors[..., :half_width]
    second_half = vectors[..., half_width:]
    cosine = jnp.cos(phases)
    sine = jnp.sin(phases)
    return jnp.concatenate(
        [first_half * cosine - second_half * sine, second_half * cosine + first_half * sine],
        axis=-1,
    )


def rope_phases(positions, width):
    inverse = 1.0 / rope_base ** (jnp.arange(0, width, 2, dtype=jnp.float32) / width)
    return positions.astype(jnp.float32)[:, None] * inverse[None, :]


def rms_scale(vectors, gain_vec):
    return (
        vectors
        * lax.rsqrt(jnp.mean(vectors * vectors, axis=-1, keepdims=True) + epsilon)
        * gain_vec
    )


def attend_block(carry, queries, key_nope, value_rows, key_rot):
    row_peak, denominator, accum = carry
    key_count = key_nope.shape[0]
    heads = queries.shape[1]
    key_all = jnp.concatenate(
        [key_nope, jnp.broadcast_to(key_rot[:, None, :], (key_count, heads, key_rot.shape[1]))],
        axis=2,
    )
    scores = jnp.einsum("qhd,khd->hqk", queries, key_all, preferred_element_type=jnp.float32) * (
        1.0 / math.sqrt(UNROTATED_WIDTH + ROPE)
    )
    new_peak = jnp.maximum(row_peak, jnp.max(scores, axis=2))
    factor = jnp.exp(row_peak - new_peak)
    weights = jnp.exp(scores - new_peak[:, :, None])
    denominator = denominator * factor + jnp.sum(weights, axis=2)
    accum = accum * jnp.transpose(factor)[:, :, None] + jnp.einsum(
        "hqk,khd->qhd", weights.astype(jnp.bfloat16), value_rows, preferred_element_type=jnp.float32
    )
    return (new_peak, denominator, accum)


def fold_blocks(carry, pieces, expand, queries):
    count = pieces[0].shape[0]
    width = math.gcd(count, 1024)

    def one_block(state, start):
        sliced = tuple((lax.dynamic_slice_in_dim(member, start, width, 0) for member in pieces))
        key_nope, value_rows, key_rot = expand(sliced)
        return attend_block(state, queries, key_nope, value_rows, key_rot)

    return lax.fori_loop(
        0, count // width, lambda turn, state: one_block(state, turn * width), carry
    )


def on_device(
    residual_in,
    queries_nope,
    queries_rope,
    latents,
    rope_keys,
    latent_norm_gain,
    key_up_weight,
    value_up_weight,
    w_out,
    norm_gain,
    w_up,
    w_down,
):
    rows = residual_in.shape[0]
    heads = key_up_weight.shape[1] // UNROTATED_WIDTH
    value_width = value_up_weight.shape[1] // heads
    positions = lax.axis_index("sp") * rows + jnp.arange(rows, dtype=jnp.int32)
    phases = rope_phases(positions, ROPE)
    q_rot = rotate(
        queries_rope.astype(jnp.float32).reshape(rows, heads, ROPE), phases[:, None, :]
    ).astype(jnp.bfloat16)
    queries = jnp.concatenate([queries_nope.reshape(rows, heads, UNROTATED_WIDTH), q_rot], axis=2)
    lat_norm = rms_scale(latents.astype(jnp.float32), latent_norm_gain).astype(jnp.bfloat16)
    key_rot = rotate(rope_keys.astype(jnp.float32), phases).astype(jnp.bfloat16)
    start_carry = (
        jnp.full((heads, rows), -1e30, jnp.float32),
        jnp.zeros((heads, rows), jnp.float32),
        jnp.zeros((rows, heads, value_width), jnp.float32),
    )

    def expand_latent(sliced):
        lat_rows, rot_rows = sliced
        count = lat_rows.shape[0]
        key_nope = (
            jnp.dot(lat_rows, key_up_weight, preferred_element_type=jnp.float32)
            .astype(jnp.bfloat16)
            .reshape(count, heads, UNROTATED_WIDTH)
        )
        value_rows = (
            jnp.dot(lat_rows, value_up_weight, preferred_element_type=jnp.float32)
            .astype(jnp.bfloat16)
            .reshape(count, heads, value_width)
        )
        return (key_nope, value_rows, rot_rows)

    result = fold_blocks(
        start_carry,
        (
            lax.all_gather(lat_norm, "sp", axis=0, tiled=True),
            lax.all_gather(key_rot, "sp", axis=0, tiled=True),
        ),
        expand_latent,
        queries,
    )
    row_peak, denominator, accum = result
    attended = (
        (accum / jnp.transpose(denominator)[:, :, None])
        .astype(jnp.bfloat16)
        .reshape(rows, heads * value_width)
    )
    part_term = jnp.dot(attended, w_out, preferred_element_type=jnp.float32)
    summed = lax.psum(part_term.astype(jnp.bfloat16), "tp").astype(jnp.float32)
    stream = residual_in.astype(jnp.float32) + summed
    normed = rms_scale(stream, norm_gain).astype(jnp.bfloat16)
    upward = jnp.dot(
        normed, lax.all_gather(w_up, "sp", axis=0, tiled=True), preferred_element_type=jnp.float32
    )
    hidden = jnp.square(jax.nn.relu(upward)).astype(jnp.bfloat16)
    terms = jnp.dot(
        hidden, lax.all_gather(w_down, "sp", axis=1, tiled=True), preferred_element_type=jnp.float32
    )
    mixer = lax.psum_scatter(
        terms.astype(jnp.bfloat16), "tp", scatter_dimension=1, tiled=True
    ).astype(jnp.float32)
    own_width = mixer.shape[1]
    own_stream = lax.dynamic_slice_in_dim(stream, lax.axis_index("tp") * own_width, own_width, 1)
    return (own_stream + mixer).astype(jnp.bfloat16)


def solution(mesh):
    in_specs = (
        P("sp", None),
        P("sp", "tp"),
        P("sp", "tp"),
        P("sp", None),
        P("sp", None),
        P(),
        P(None, "tp"),
        P(None, "tp"),
        P("tp", None),
        P(),
        P("sp", "tp"),
        P("tp", "sp"),
    )
    out_specs = P("sp", "tp")
    return jax.shard_map(
        on_device, mesh=mesh, in_specs=in_specs, out_specs=out_specs, check_vma=False
    )
```

profile of v0, /device:TPU:0, one launch (start us, length us, event | category | flops | bytes accessed | tf_op | source)
XLA Modules:
  0.0 480.2 jit_solution(10684508900544184789)
XLA Ops:
  7.7 1.8 fusion.27
  12.8 33.2 %all_gather.13 = bf16[4096,32]{0,1:T(8,128)(2,1)S(1)} all-gather(bf16[512,32]{0,1:T(8,128)(2,1)S(1)} %pad_maximum_fusion.1), channel_id=1, replica_groups=mesh['sp'=8,'tp'=4] {'sp'}, dimensions={0}, use_global_device_ids=true | all-gather | bytes 294912 | tf_op jit(solution)/shard_map/all_gather | solution.py:123
  46.0 16.1 %all-gather.4.cloned.1.call-done = bf16[4096,256]{1,0:T(8,128)(2,1)} async-done(((bf16[512,256]{1,0:T(8,128)(2,1)}), bf16[4096,256]{1,0:T(8,128)(2,1)}) %all-gather.4.cloned.1.call-update) | async-done | bytes 2097168 | tf_op jit(solution)/shard_map/all_gather | solution.py:122
  62.1 58.6 %while.18 = (s32[]{:T(128)}, f32[4,512]{1,0:T(4,128)S(1)}, f32[4,512]{1,0:T(4,128)S(1)}, f32[512,4,64]{0,2,1:T(8,128)S(1)}, bf16[4096,256]{1,0:T(8,128)(2,1)}, /...) while((s32[]{:T(128)}, f32[4,512]{1,0:T(4,128)S(1)}, ...), condition=%wide.region_4.0_spmd.clone, body=%wide.region_1.0_spmd.clone.sunk | while | flops 958803968 | bytes 64946424 | solution.py:68
  62.1 1.4 convolution_convert_fusion.6
  63.6 4.5 bitcast_reduce_fusion.2
  69.6 5.1 %fusion.62 = f32[512,4,64]{0,2,1:T(8,128)S(1)} fusion(bf16[1024,4,64]{0,2,1:T(8,128)(2,1)S(1)} %bitcast.61, f32[4,1024,512]{2,1,0:T(8,128)} %get-tuple-element.285, f32[4,512]{1,0:T(4,128)S(1)} %get-tuple-element.314, f32[512,4,64]{0,2,1:T(8,128)S(1)} %get-tuple-element.303, f32[512,4]{0,1:T(4,128)S(1)} %get-tuple-element.286, pred[]{:T(512)S(6)} %compare.3), kind=kOutput, calls=%fused_computation.9.clone.1 | convolution fusion | flops 275120128 | bytes 9977857 | tf_op jit(solution)/shard_map/while/body/eval_jaxpr/hqk,khd->qhd/dot_general | solution.py:53
  76.8 1.4 convolution_convert_fusion.6
  78.3 4.5 bitcast_reduce_fusion.2
  84.2 5.1 %fusion.62 = f32[512,4,64]{0,2,1:T(8,128)S(1)} fusion(bf16[1024,4,64]{0,2,1:T(8,128)(2,1)S(1)} %bitcast.61, f32[4,1024,512]{2,1,0:T(8,128)} %get-tuple-element.285, f32[4,512]{1,0:T(4,128)S(1)} %get-tuple-element.314, f32[512,4,64]{0,2,1:T(8,128)S(1)} %get-tuple-element.303, f32[512,4]{0,1:T(4,128)S(1)} %get-tuple-element.286, pred[]{:T(512)S(6)} %compare.3), kind=kOutput, calls=%fused_computation.9.clone.1 | convolution fusion | flops 275120128 | bytes 9977857 | tf_op jit(solution)/shard_map/while/body/eval_jaxpr/hqk,khd->qhd/dot_general | solution.py:53
  91.4 1.4 convolution_convert_fusion.6
  92.9 4.5 bitcast_reduce_fusion.2
  98.9 5.1 %fusion.62 = f32[512,4,64]{0,2,1:T(8,128)S(1)} fusion(bf16[1024,4,64]{0,2,1:T(8,128)(2,1)S(1)} %bitcast.61, f32[4,1024,512]{2,1,0:T(8,128)} %get-tuple-element.285, f32[4,512]{1,0:T(4,128)S(1)} %get-tuple-element.314, f32[512,4,64]{0,2,1:T(8,128)S(1)} %get-tuple-element.303, f32[512,4]{0,1:T(4,128)S(1)} %get-tuple-element.286, pred[]{:T(512)S(6)} %compare.3), kind=kOutput, calls=%fused_computation.9.clone.1 | convolution fusion | flops 275120128 | bytes 9977857 | tf_op jit(solution)/shard_map/while/body/eval_jaxpr/hqk,khd->qhd/dot_general | solution.py:53
  106.1 1.4 convolution_convert_fusion.6
  107.6 4.5 bitcast_reduce_fusion.2
  113.5 5.1 %fusion.62 = f32[512,4,64]{0,2,1:T(8,128)S(1)} fusion(bf16[1024,4,64]{0,2,1:T(8,128)(2,1)S(1)} %bitcast.61, f32[4,1024,512]{2,1,0:T(8,128)} %get-tuple-element.285, f32[4,512]{1,0:T(4,128)S(1)} %get-tuple-element.314, f32[512,4,64]{0,2,1:T(8,128)S(1)} %get-tuple-element.303, f32[512,4]{0,1:T(4,128)S(1)} %get-tuple-element.286, pred[]{:T(512)S(6)} %compare.3), kind=kOutput, calls=%fused_computation.9.clone.1 | convolution fusion | flops 275120128 | bytes 9977857 | tf_op jit(solution)/shard_map/while/body/eval_jaxpr/hqk,khd->qhd/dot_general | solution.py:53
  120.8 2.1 convolution_convert_fusion.2
  124.5 48.9 %all-reduce.2.cloned.1.call-done = bf16[512,2048]{1,0:T(8,128)(2,1)} async-done(((bf16[512,2048]{1,0:T(8,128)(2,1)}), bf16[512,2048]{1,0:T(8,128)(2,1)}) %all-reduce.2.cloned.1.call-update) | async-done | bytes 2097168 | tf_op jit(solution)/shard_map/psum | solution.py:135
  173.4 4.2 convert_add_fusion
  177.6 122.5 %all-gather.6.cloned.1.call-done = bf16[2048,2048]{1,0:T(8,128)(2,1)} async-done(((bf16[256,2048]{1,0:T(8,128)(2,1)}), bf16[2048,2048]{1,0:T(8,128)(2,1)}) %all-gather.6.cloned.1.call-update) | async-done | bytes 8388624 | tf_op jit(solution)/shard_map/all_gather | solution.py:139
  300.1 125.0 %all-gather.8.cloned.1.call-done = bf16[2048,2048]{1,0:T(8,128)(2,1)} async-done(((bf16[2048,256]{1,0:T(8,128)(2,1)}), bf16[2048,2048]{1,0:T(8,128)(2,1)}) %all-gather.8.cloned.1.call-update) | async-done | bytes 8388624 | tf_op jit(solution)/shard_map/all_gather | solution.py:143
  425.2 16.6 %convolution_convert_fusion.3 = bf16[512,2048]{1,0:T(8,128)(2,1)} fusion(bf16[2048,2048]{1,0:T(8,128)(2,1)} %all-gather.8.cloned.1.call-done, bf16[2048,2048]{1,0:T(8,128)(2,1)} %all-gather.6.cloned.1.call-done, f32[2048]{0:T(1024)S(1)} %copy-done.4, f32[512]{0:T(512)S(1)} %add_rsqrt_fusion, bf16[512,2048]{1,0:T(8,128)(2,1)} %all-reduce.2.cloned.1.call-done, ...), kind=kOutput, calls=%fused_computation.32 | convolution fusion | flops 8600420352 | bytes 23078912 | tf_op jit(solution)/shard_map/dot_general | solution.py:142
  441.8 29.5 %reduce-scatter.2.cloned.1.call-done = bf16[512,512]{1,0:T(8,128)(2,1)} async-done(((bf16[512,2048]{1,0:T(8,128)(2,1)}), bf16[512,512]{1,0:T(8,128)(2,1)}) %reduce-scatter.2.cloned.1.call-update) | async-done | bytes 524304 | tf_op jit(solution)/shard_map/reduce_scatter | solution.py:145
  471.3 2.3 add_convert_fusion
  (76 shorter events, 19.8 us)
Async XLA Ops:
  6.5 114.3 %copy-start = (bf16[256,2048]{1,0:T(8,128)(2,1)S(1)}, bf16[256,2048]{1,0:T(8,128)(2,1)}, u32[]{:S(2)}) copy-start(bf16[256,2048]{1,0:T(8,128)(2,1)} %param.22) | copy-start | bytes 3145732
  6.5 55.6 %all-gather.4.cloned.1.call-start = ((), (), s32[]{:S(2)}) async-start(), calls=%async_computation.1 | async-start | bytes 2359296 | tf_op jit(solution)/shard_map/all_gather | solution.py:122
  9.6 163.9 %all-reduce.2.cloned.1.call-start = ((), (), s32[]{:S(2)}) async-start(), calls=%async_computation.2 | async-start | bytes 4194304 | tf_op jit(solution)/shard_map/psum | solution.py:135
  63.6 4.6 copy-start.2
  69.6 5.8 %copy-start.1 = (f32[4,1024,512]{2,1,0:T(8,128)S(1)}, f32[4,1024,512]{2,1,0:T(8,128)}, u32[]{:S(2)}) copy-start(f32[4,1024,512]{2,1,0:T(8,128)} %get-tuple-element.285) | copy-start | bytes 25165828 | tf_op jit(solution)/shard_map/while
  78.2 4.6 copy-start.2
  84.2 5.8 %copy-start.1 = (f32[4,1024,512]{2,1,0:T(8,128)S(1)}, f32[4,1024,512]{2,1,0:T(8,128)}, u32[]{:S(2)}) copy-start(f32[4,1024,512]{2,1,0:T(8,128)} %get-tuple-element.285) | copy-start | bytes 25165828 | tf_op jit(solution)/shard_map/while
  92.9 4.6 copy-start.2
  98.9 5.8 %copy-start.1 = (f32[4,1024,512]{2,1,0:T(8,128)S(1)}, f32[4,1024,512]{2,1,0:T(8,128)}, u32[]{:S(2)}) copy-start(f32[4,1024,512]{2,1,0:T(8,128)} %get-tuple-element.285) | copy-start | bytes 25165828 | tf_op jit(solution)/shard_map/while
  107.5 4.6 copy-start.2
  113.5 5.8 %copy-start.1 = (f32[4,1024,512]{2,1,0:T(8,128)S(1)}, f32[4,1024,512]{2,1,0:T(8,128)}, u32[]{:S(2)}) copy-start(f32[4,1024,512]{2,1,0:T(8,128)} %get-tuple-element.285) | copy-start | bytes 25165828 | tf_op jit(solution)/shard_map/while
  120.8 52.6 %copy-start.3 = (bf16[512,2048]{1,0:T(8,128)(2,1)S(1)}, bf16[512,2048]{1,0:T(8,128)(2,1)}, u32[]{:S(2)}) copy-start(bf16[512,2048]{1,0:T(8,128)(2,1)} %param.14) | copy-start | bytes 6291460
  122.9 177.2 %all-gather.6.cloned.1.call-start = ((), (), s32[]{:S(2)}) async-start(), calls=%async_computation.3 | async-start | bytes 9437184 | tf_op jit(solution)/shard_map/all_gather | solution.py:139
  123.7 301.5 %all-gather.8.cloned.1.call-start = ((), (), s32[]{:S(2)}) async-start(), calls=%async_computation.4 | async-start | bytes 9437184 | tf_op jit(solution)/shard_map/all_gather | solution.py:143
  124.2 300.9 %copy-start.4 = (f32[2048]{0:T(1024)S(1)}, f32[2048]{0:T(1024)}, u32[]{:S(2)}) copy-start(f32[2048]{0:T(1024)} %param.23) | copy-start | bytes 24580
  124.3 347.1 %reduce-scatter.2.cloned.1.call-start = ((), (), s32[]{:S(2)}) async-start(), calls=%async_computation.5 | async-start | bytes 2621440 | tf_op jit(solution)/shard_map/reduce_scatter | solution.py:145
Sparse Core Ops, SparseCore 0:
  9.7 52.4 all-gather.3
  123.0 50.3 all-reduce.1
  175.6 124.5 all-gather.5
  302.0 123.1 all-gather.7
  441.9 29.3 reduce-scatter.1
where the time goes:
time: 481 us; the launch traced here: 480 us
  waiting for transfers between devices  343 us (71%)
  matrix products  68.6 us (14%)
  blocking collectives  33.2 us (7%)
  other arithmetic  16.3 us (3%)
  between operations  13.3 us (3%)
    all_gather x1, waiting for transfers between devices, on_device(): lax.all_gather(w_down, 'sp', axis=1, tiled=True)  125 us
    all_gather x1, waiting for transfers between devices, on_device(): lax.all_gather(w_up, 'sp', axis=0, tiled=True)  123 us
    psum x1, waiting for transfers between devices, on_device(): summed = lax.psum(part_term.astype(jnp.bfloat16), 'tp').astype(jnp.float32)  48.9 us
    all_gather x1, blocking collectives, on_device(): lax.all_gather(key_rot, 'sp', axis=0, tiled=True)  33.2 us
    reduce_scatter x1, waiting for transfers between devices, on_device(): lax.psum_scatter(terms.astype(jnp.bfloat16), 'tp', scatter_dimension=1, t...  29.5 us
    dot_general x4, matrix products, attend_block(): jnp.einsum('hqk,khd->qhd', weights.astype(jnp.bfloat16), value_rows, pref...  20.6 us
    dot_general x4, matrix products, attend_block(): jnp.einsum('qhd,khd->hqk', queries, key_all, preferred_element_type=jnp.f...  18.2 us
    dot_general x1, matrix products, on_device(): jnp.dot(hidden, lax.all_gather(w_down, 'sp', axis=1, tiled=True), preferr...  16.6 us
  transfers between devices with their start and end apart: 5, of which 5 were waited for; matrix products, arithmetic and copies ran while one was open for 2% of the time, Pallas kernels for 0%

commit v1 on v0

--- a/solution.py
+++ b/solution.py
@@ -120,7 +120,15 @@
         start_carry,
         (
             lax.all_gather(lat_norm, "sp", axis=0, tiled=True),
-            lax.all_gather(key_rot, "sp", axis=0, tiled=True),
+            jnp.concatenate(
+                lax.all_to_all(
+                    jnp.stack([key_rot for _ in range(lax.axis_size("sp"))], axis=0),
+                    axis_name="sp",
+                    split_axis=0,
+                    concat_axis=0,
+                ),
+                0,
+            ),
         ),
         expand_latent,
         queries,

time: 481 us -> 483 us (level)
  blocking collectives: 33.2 us -> 0 us
  waiting for transfers between devices: 343 us -> 370 us
  starting transfers between devices: 0.34 us -> 7.65 us
    all_gather x1 -> x0, blocking collectives: 33.2 us -> none  [on_device(): lax.all_gather(key_rot, 'sp', axis=0, tiled=True)]
    all_gather x1, waiting for transfers between devices: 16.1 us -> 31.7 us  [on_device(): lax.all_gather(lat_norm, 'sp', axis=0, tiled=True)]
    all_to_all x0 -> x1, waiting for transfers between devices: none -> 11.7 us  [on_device(): lax.all_to_all(jnp.stack([key_rot for _ in range(lax.axis_size('sp'))], a...]
    all_to_all x0 -> x1, starting transfers between devices: none -> 7.31 us  [on_device(): lax.all_to_all(jnp.stack([key_rot for _ in range(lax.axis_size('sp'))], a...]
  transfers between devices with their start and end apart: 5 -> 6, of which waited for: 5 -> 6; matrix products, arithmetic and copies ran while one was open for 2% -> 2% of each run, Pallas kernels for 0% -> 0%
where the time goes in v1:
time: 483 us; the launch traced here: 482 us
  waiting for transfers between devices  370 us (77%)
  matrix products  68.5 us (14%)
  other arithmetic  16.3 us (3%)
  between operations  13.3 us (3%)
  starting transfers between devices  7.65 us (2%)
  local copies, waits for them, and re-layouts  5.46 us (1%)
    all_gather x1, waiting for transfers between devices, on_device(): lax.all_gather(w_down, 'sp', axis=1, tiled=True)  125 us
    all_gather x1, waiting for transfers between devices, on_device(): lax.all_gather(w_up, 'sp', axis=0, tiled=True)  123 us
    psum x1, waiting for transfers between devices, on_device(): summed = lax.psum(part_term.astype(jnp.bfloat16), 'tp').astype(jnp.float32)  48.5 us
    all_gather x1, waiting for transfers between devices, on_device(): lax.all_gather(lat_norm, 'sp', axis=0, tiled=True)  31.7 us
    reduce_scatter x1, waiting for transfers between devices, on_device(): lax.psum_scatter(terms.astype(jnp.bfloat16), 'tp', scatter_dimension=1, t...  29.5 us
    dot_general x4, matrix products, attend_block(): jnp.einsum('hqk,khd->qhd', weights.astype(jnp.bfloat16), value_rows, pref...  20.6 us
    dot_general x4, matrix products, attend_block(): jnp.einsum('qhd,khd->hqk', queries, key_all, preferred_element_type=jnp.f...  18.1 us
    dot_general x1, matrix products, on_device(): jnp.dot(hidden, lax.all_gather(w_down, 'sp', axis=1, tiled=True), preferr...  16.6 us
  transfers between devices with their start and end apart: 6, of which 6 were waited for; matrix products, arithmetic and copies ran while one was open for 2% of the time, Pallas kernels for 0%

profile of v1, /device:TPU:0, one launch (start us, length us, event | category | flops | bytes accessed | tf_op | source)
XLA Modules:
  0.0 481.8 jit_solution(5439868228983769763)
XLA Ops:
  7.8 1.8 fusion.27
  11.3 7.3 %all-to-all-start = ((bf16[8,512,32]{1,2,0:T(8,128)(2,1)}), bf16[8,512,32]{1,2,0:T(8,128)(2,1)S(1)}, u32[]{:S(2)}, u32[]{:S(2)}) async-start(bf16[8,512,32]{1,2,0:T(8,128)(2,1)} %stack.2), calls=%async_computation | async-start | bytes 524288 | tf_op jit(solution)/shard_map/all_to_all | solution.py:124
  20.9 11.7 %all-to-all-done = bf16[8,512,32]{1,2,0:T(8,128)(2,1)S(1)} async-done(((bf16[8,512,32]{1,2,0:T(8,128)(2,1)}), bf16[8,512,32]{1,2,0:T(8,128)(2,1)S(1)}, u32[]{:S(2)}, u32[]{:S(2)}) %all-to-all-start) | async-done | bytes 262176 | tf_op jit(solution)/shard_map/all_to_all | solution.py:124
  32.6 31.7 %all-gather.4.cloned.1.call-done = bf16[4096,256]{1,0:T(8,128)(2,1)} async-done(((bf16[512,256]{1,0:T(8,128)(2,1)}), bf16[4096,256]{1,0:T(8,128)(2,1)}) %all-gather.4.cloned.1.call-update) | async-done | bytes 2097168 | tf_op jit(solution)/shard_map/all_gather | solution.py:122
  64.4 58.4 %while.18 = (s32[]{:T(128)}, f32[4,512]{1,0:T(4,128)S(1)}, f32[4,512]{1,0:T(4,128)S(1)}, f32[512,4,64]{0,2,1:T(8,128)S(1)}, bf16[4096,256]{1,0:T(8,128)(2,1)}, /...) while((s32[]{:T(128)}, f32[4,512]{1,0:T(4,128)S(1)}, ...), condition=%wide.region_4.0_spmd.clone, body=%wide.region_1.0_spmd.clone.sunk | while | flops 958803968 | bytes 64422108 | solution.py:68
  65.8 4.5 bitcast_reduce_fusion.2
  70.4 1.4 convolution_convert_fusion.7
  71.8 5.1 %fusion.62 = f32[512,4,64]{0,2,1:T(8,128)S(1)} fusion(bf16[1024,4,64]{0,2,1:T(8,128)(2,1)S(1)} %bitcast.63, f32[4,1024,512]{2,1,0:T(8,128)} %get-tuple-element.285, f32[4,512]{1,0:T(4,128)S(1)} %get-tuple-element.314, f32[512,4,64]{0,2,1:T(8,128)S(1)} %get-tuple-element.303, f32[512,4]{0,1:T(4,128)S(1)} %get-tuple-element.286, pred[]{:T(512)S(6)} %compare.3), kind=kOutput, calls=%fused_computation.9.clone.1 | convolution fusion | flops 275120128 | bytes 9977857 | tf_op jit(solution)/shard_map/while/body/eval_jaxpr/hqk,khd->qhd/dot_general | solution.py:53
  80.4 4.5 bitcast_reduce_fusion.2
  86.4 5.1 %fusion.62 = f32[512,4,64]{0,2,1:T(8,128)S(1)} fusion(bf16[1024,4,64]{0,2,1:T(8,128)(2,1)S(1)} %bitcast.63, f32[4,1024,512]{2,1,0:T(8,128)} %get-tuple-element.285, f32[4,512]{1,0:T(4,128)S(1)} %get-tuple-element.314, f32[512,4,64]{0,2,1:T(8,128)S(1)} %get-tuple-element.303, f32[512,4]{0,1:T(4,128)S(1)} %get-tuple-element.286, pred[]{:T(512)S(6)} %compare.3), kind=kOutput, calls=%fused_computation.9.clone.1 | convolution fusion | flops 275120128 | bytes 9977857 | tf_op jit(solution)/shard_map/while/body/eval_jaxpr/hqk,khd->qhd/dot_general | solution.py:53
  95.0 4.5 bitcast_reduce_fusion.2
  99.5 1.4 convolution_convert_fusion.7
  100.9 5.1 %fusion.62 = f32[512,4,64]{0,2,1:T(8,128)S(1)} fusion(bf16[1024,4,64]{0,2,1:T(8,128)(2,1)S(1)} %bitcast.63, f32[4,1024,512]{2,1,0:T(8,128)} %get-tuple-element.285, f32[4,512]{1,0:T(4,128)S(1)} %get-tuple-element.314, f32[512,4,64]{0,2,1:T(8,128)S(1)} %get-tuple-element.303, f32[512,4]{0,1:T(4,128)S(1)} %get-tuple-element.286, pred[]{:T(512)S(6)} %compare.3), kind=kOutput, calls=%fused_computation.9.clone.1 | convolution fusion | flops 275120128 | bytes 9977857 | tf_op jit(solution)/shard_map/while/body/eval_jaxpr/hqk,khd->qhd/dot_general | solution.py:53
  109.6 4.5 bitcast_reduce_fusion.2
  114.1 1.4 convolution_convert_fusion.7
  115.5 5.1 %fusion.62 = f32[512,4,64]{0,2,1:T(8,128)S(1)} fusion(bf16[1024,4,64]{0,2,1:T(8,128)(2,1)S(1)} %bitcast.63, f32[4,1024,512]{2,1,0:T(8,128)} %get-tuple-element.285, f32[4,512]{1,0:T(4,128)S(1)} %get-tuple-element.314, f32[512,4,64]{0,2,1:T(8,128)S(1)} %get-tuple-element.303, f32[512,4]{0,1:T(4,128)S(1)} %get-tuple-element.286, pred[]{:T(512)S(6)} %compare.3), kind=kOutput, calls=%fused_computation.9.clone.1 | convolution fusion | flops 275120128 | bytes 9977857 | tf_op jit(solution)/shard_map/while/body/eval_jaxpr/hqk,khd->qhd/dot_general | solution.py:53
  122.8 2.1 convolution_convert_fusion.2
  126.5 48.5 %all-reduce.2.cloned.1.call-done = bf16[512,2048]{1,0:T(8,128)(2,1)} async-done(((bf16[512,2048]{1,0:T(8,128)(2,1)}), bf16[512,2048]{1,0:T(8,128)(2,1)}) %all-reduce.2.cloned.1.call-update) | async-done | bytes 2097168 | tf_op jit(solution)/shard_map/psum | solution.py:143
  175.0 4.2 convert_add_fusion
  179.2 122.5 %all-gather.6.cloned.1.call-done = bf16[2048,2048]{1,0:T(8,128)(2,1)} async-done(((bf16[256,2048]{1,0:T(8,128)(2,1)}), bf16[2048,2048]{1,0:T(8,128)(2,1)}) %all-gather.6.cloned.1.call-update) | async-done | bytes 8388624 | tf_op jit(solution)/shard_map/all_gather | solution.py:147
  301.7 125.0 %all-gather.8.cloned.1.call-done = bf16[2048,2048]{1,0:T(8,128)(2,1)} async-done(((bf16[2048,256]{1,0:T(8,128)(2,1)}), bf16[2048,2048]{1,0:T(8,128)(2,1)}) %all-gather.8.cloned.1.call-update) | async-done | bytes 8388624 | tf_op jit(solution)/shard_map/all_gather | solution.py:151
  426.8 16.6 %convolution_convert_fusion.3 = bf16[512,2048]{1,0:T(8,128)(2,1)} fusion(bf16[2048,2048]{1,0:T(8,128)(2,1)} %all-gather.8.cloned.1.call-done, bf16[2048,2048]{1,0:T(8,128)(2,1)} %all-gather.6.cloned.1.call-done, f32[2048]{0:T(1024)S(1)} %copy-done.5, f32[512]{0:T(512)S(1)} %add_rsqrt_fusion, bf16[512,2048]{1,0:T(8,128)(2,1)} %all-reduce.2.cloned.1.call-done, ...), kind=kOutput, calls=%fused_computation.32 | convolution fusion | flops 8600420352 | bytes 23078912 | tf_op jit(solution)/shard_map/dot_general | solution.py:150
  443.4 29.5 %reduce-scatter.2.cloned.1.call-done = bf16[512,512]{1,0:T(8,128)(2,1)} async-done(((bf16[512,2048]{1,0:T(8,128)(2,1)}), bf16[512,512]{1,0:T(8,128)(2,1)}) %reduce-scatter.2.cloned.1.call-update) | async-done | bytes 524304 | tf_op jit(solution)/shard_map/reduce_scatter | solution.py:153
  472.9 2.3 add_convert_fusion
  (75 shorter events, 22.0 us)
Async XLA Ops:
  6.5 116.3 %copy-start = (bf16[256,2048]{1,0:T(8,128)(2,1)S(1)}, bf16[256,2048]{1,0:T(8,128)(2,1)}, u32[]{:S(2)}) copy-start(bf16[256,2048]{1,0:T(8,128)(2,1)} %param.22) | copy-start | bytes 3145732
  6.5 57.8 %copy-start.2 = (bf16[256,256]{1,0:T(8,128)(2,1)S(1)}, bf16[256,256]{1,0:T(8,128)(2,1)}, u32[]{:S(2)}) copy-start(bf16[256,256]{1,0:T(8,128)(2,1)} %param.20) | copy-start | bytes 393220
  6.5 57.8 %copy-start.3 = (bf16[256,256]{1,0:T(8,128)(2,1)S(1)}, bf16[256,256]{1,0:T(8,128)(2,1)}, u32[]{:S(2)}) copy-start(bf16[256,256]{1,0:T(8,128)(2,1)} %param.21) | copy-start | bytes 393220
  6.5 57.8 %all-gather.4.cloned.1.call-start = ((), (), s32[]{:S(2)}) async-start(), calls=%async_computation.2 | async-start | bytes 2359296 | tf_op jit(solution)/shard_map/all_gather | solution.py:122
  11.3 21.3 %all-to-all-start = ((bf16[8,512,32]{1,2,0:T(8,128)(2,1)}), bf16[8,512,32]{1,2,0:T(8,128)(2,1)S(1)}, u32[]{:S(2)}, u32[]{:S(2)}) async-start(bf16[8,512,32]{1,2,0:T(8,128)(2,1)} %stack.2), calls=%async_computation | async-start | bytes 524288 | tf_op jit(solution)/shard_map/all_to_all | solution.py:124
  18.6 156.4 %all-reduce.2.cloned.1.call-start = ((), (), s32[]{:S(2)}) async-start(), calls=%async_computation.3 | async-start | bytes 4194304 | tf_op jit(solution)/shard_map/psum | solution.py:143
  71.8 5.8 %copy-start.1 = (f32[4,1024,512]{2,1,0:T(8,128)S(1)}, f32[4,1024,512]{2,1,0:T(8,128)}, u32[]{:S(2)}) copy-start(f32[4,1024,512]{2,1,0:T(8,128)} %get-tuple-element.285) | copy-start | bytes 25165828 | tf_op jit(solution)/shard_map/while
  86.3 5.8 %copy-start.1 = (f32[4,1024,512]{2,1,0:T(8,128)S(1)}, f32[4,1024,512]{2,1,0:T(8,128)}, u32[]{:S(2)}) copy-start(f32[4,1024,512]{2,1,0:T(8,128)} %get-tuple-element.285) | copy-start | bytes 25165828 | tf_op jit(solution)/shard_map/while
  100.9 5.8 %copy-start.1 = (f32[4,1024,512]{2,1,0:T(8,128)S(1)}, f32[4,1024,512]{2,1,0:T(8,128)}, u32[]{:S(2)}) copy-start(f32[4,1024,512]{2,1,0:T(8,128)} %get-tuple-element.285) | copy-start | bytes 25165828 | tf_op jit(solution)/shard_map/while
  115.5 5.8 %copy-start.1 = (f32[4,1024,512]{2,1,0:T(8,128)S(1)}, f32[4,1024,512]{2,1,0:T(8,128)}, u32[]{:S(2)}) copy-start(f32[4,1024,512]{2,1,0:T(8,128)} %get-tuple-element.285) | copy-start | bytes 25165828 | tf_op jit(solution)/shard_map/while
  122.8 52.2 %copy-start.4 = (bf16[512,2048]{1,0:T(8,128)(2,1)S(1)}, bf16[512,2048]{1,0:T(8,128)(2,1)}, u32[]{:S(2)}) copy-start(bf16[512,2048]{1,0:T(8,128)(2,1)} %param.14) | copy-start | bytes 6291460
  124.9 176.8 %all-gather.6.cloned.1.call-start = ((), (), s32[]{:S(2)}) async-start(), calls=%async_computation.4 | async-start | bytes 9437184 | tf_op jit(solution)/shard_map/all_gather | solution.py:147
  125.7 301.1 %all-gather.8.cloned.1.call-start = ((), (), s32[]{:S(2)}) async-start(), calls=%async_computation.5 | async-start | bytes 9437184 | tf_op jit(solution)/shard_map/all_gather | solution.py:151
  126.2 300.5 %copy-start.5 = (f32[2048]{0:T(1024)S(1)}, f32[2048]{0:T(1024)}, u32[]{:S(2)}) copy-start(f32[2048]{0:T(1024)} %param.23) | copy-start | bytes 24580
  126.2 346.6 %reduce-scatter.2.cloned.1.call-start = ((), (), s32[]{:S(2)}) async-start(), calls=%async_computation.6 | async-start | bytes 2621440 | tf_op jit(solution)/shard_map/reduce_scatter | solution.py:153
Sparse Core Ops, SparseCore 0:
  9.7 54.6 all-gather.3
  125.0 49.9 all-reduce.1
  177.1 124.5 all-gather.5
  303.6 123.1 all-gather.7
  443.5 29.3 reduce-scatter.1
